TPU v7x, 32 devices: a whole 2x2x4 slice. The times are simulated.
32 devices in a mesh: ep: 8 (over z, x), tp: 4 (over y, core).
Axes of the slice: x: 2, y: 2, z: 4, core: 2. Of those that a mesh axis runs over, the one named last changes fastest.
Arguments:
- tokens: bfloat16 [768, 4096], P('ep'), may hold values from -6 to 6
- mix_gain: float32 [4096], replicated, may hold values from 0.1 to 1.9
- ffn_gain: float32 [4096], replicated, may hold values from 0.1 to 1.9
- in_proj: bfloat16 [4096, 1024], P(None, 'tp'), may hold values from -0.09375 to 0.09375
- decay_rate: float32 [64, 64], P('tp'), may hold values from 0.05 to 2
- frequency: float32 [64, 64], P('tp'), may hold values from -3 to 3
- log_step: float32 [64], P('tp'), may hold values from -3 to 0.5
- b_real: float32 [64, 64, 16], P('tp'), may hold values from -1.5 to 1.5
- b_imag: float32 [64, 64, 16], P('tp'), may hold values from -1.5 to 1.5
- c_real: float32 [64, 16, 64], P('tp'), may hold values from -0.75 to 0.75
- c_imag: float32 [64, 16, 64], P('tp'), may hold values from -0.75 to 0.75
- skip_gain: float32 [1024], P('tp'), may hold values from -5 to 5
- states: float32 [2, 768, 4096], P(None, 'ep', 'tp'), may hold values from -6 to 6
- out_proj: bfloat16 [1024, 4096], P('tp'), may hold values from -0.1875 to 0.1875
- route_ids: int32 [768, 2], P('ep'), may hold values from 0 to 7, all different within a row; in each aligned block of 96 rows (0 to 95, 96 to 191, ...) at most 48 rows name the same one
- route_logits: float32 [768, 2], P('ep'), may hold values from -5 to 5
- expert_gate: bfloat16 [8, 4096, 3072], P('ep', None, 'tp'), may hold values from -0.09375 to 0.09375
- expert_up: bfloat16 [8, 4096, 3072], P('ep', None, 'tp'), may hold values from -0.09375 to 0.09375
- expert_down: bfloat16 [8, 3072, 4096], P('ep', 'tp'), may hold values from -0.109375 to 0.109375
- dense_gate: bfloat16 [4096, 6144], P('tp', 'ep'), may hold values from -0.09375 to 0.09375
- dense_up: bfloat16 [4096, 6144], P('tp', 'ep'), may hold values from -0.09375 to 0.09375
- dense_down: bfloat16 [6144, 4096], P('ep', 'tp'), may hold values from -0.078125 to 0.078125
- branch_gate: bfloat16 [4096], replicated, may hold values from -0.09375 to 0.09375
Outputs:
- output: bfloat16 [768, 4096], P('ep', 'tp')
- new_states: float32 [2, 768, 4096], P(None, 'ep', 'tp')
Inputs may be any that keep to these rules, and one draw needn't show every extreme that they name: `route_ids`: each row names 2 different experts; among the rows of one device (aligned blocks of 96 rows) no expert is named by more than 48 rows.
All inputs are finite; a program needn't handle non-finite values.
Results may differ from a plain program's by a relative error of at most 0.017.
Values may be sent and summed in bfloat16 or wider, within the bound.
A program may use at most 128 MiB of HBM per device.

v0:
```python
import jax
import jax.numpy as jnp
from jax import lax
from jax.sharding import PartitionSpec as P

GROUP = 16
STATE = 64


def rms_norm(values, gain):
    flt = values.astype(jnp.float32)
    scaled = flt * lax.rsqrt(jnp.mean(flt * flt, axis=-1, keepdims=True) + 1e-06)
    return (scaled * gain).astype(jnp.bfloat16)


def discretize(decay_rate, frequency, log_step, b_real, b_imag):
    step_size = jnp.exp(log_step)[:, None]
    lam_re = -decay_rate
    magnitude = jnp.exp(lam_re * step_size)
    abar_re = magnitude * jnp.cos(frequency * step_size)
    abar_im = magnitude * jnp.sin(frequency * step_size)
    denom = lam_re * lam_re + frequency * frequency
    fac_re = ((abar_re - 1.0) * lam_re + abar_im * frequency) / denom
    fac_im = (abar_im * lam_re - (abar_re - 1.0) * frequency) / denom
    bbar_re = fac_re[..., None] * b_real - fac_im[..., None] * b_imag
    bbar_im = fac_re[..., None] * b_imag + fac_im[..., None] * b_real
    return (abar_re, abar_im, bbar_re, bbar_im)


def state_step(
    drive, states, decay_rate, frequency, log_step, b_real, b_imag, c_real, c_imag, skip_gain
):
    count = drive.shape[0]
    groups = decay_rate.shape[0]
    abar_re, abar_im, bbar_re, bbar_im = discretize(decay_rate, frequency, log_step, b_real, b_imag)
    grouped = drive.astype(jnp.float32).reshape(count, groups, GROUP)
    old_re = states[0].reshape(count, groups, STATE)
    old_im = states[1].reshape(count, groups, STATE)
    high = lax.Precision.HIGHEST
    push_re = jnp.einsum("ngh,gph->ngp", grouped, bbar_re, precision=high)
    push_im = jnp.einsum("ngh,gph->ngp", grouped, bbar_im, precision=high)
    new_re = abar_re * old_re - abar_im * old_im + push_re
    new_im = abar_re * old_im + abar_im * old_re + push_im
    readout = (
        jnp.einsum("ngp,ghp->ngh", new_re, c_real, precision=high)
        - jnp.einsum("ngp,ghp->ngh", new_im, c_imag, precision=high)
        + skip_gain.reshape(groups, GROUP) * grouped
    )
    reads = jax.nn.gelu(readout.reshape(count, groups * GROUP)).astype(jnp.bfloat16)
    fresh = jnp.stack(
        [new_re.reshape(count, groups * STATE), new_im.reshape(count, groups * STATE)]
    )
    return (reads, fresh)


def expert_rows(full_rows, gate_w, up_w, down_w, part_width):
    sources, items, width = full_rows.shape
    flat_rows = full_rows.reshape(sources * items, width)
    gate_val = jnp.dot(flat_rows, gate_w, preferred_element_type=jnp.float32)
    up_val = jnp.dot(flat_rows, up_w, preferred_element_type=jnp.float32)
    hidden = (jax.nn.silu(gate_val) * up_val).astype(jnp.bfloat16)
    partial_value = (
        jnp.dot(hidden, down_w, preferred_element_type=jnp.float32)
        .astype(jnp.bfloat16)
        .astype(jnp.float32)
    )
    summed = lax.psum_scatter(
        partial_value.astype(jnp.bfloat16), "tp", scatter_dimension=1, tiled=True
    )
    return summed.reshape(sources, items, part_width)


def shards(
    tokens,
    mix_gain,
    ffn_gain,
    in_proj,
    decay_rate,
    frequency,
    log_step,
    b_real,
    b_imag,
    c_real,
    c_imag,
    skip_gain,
    states,
    out_proj,
    route_ids,
    route_logits,
    expert_gate,
    expert_up,
    expert_down,
    dense_gate,
    dense_up,
    dense_down,
    branch_gate,
):
    seq_count, width = tokens.shape
    tp_count = lax.axis_size("tp")
    ep_count = lax.axis_size("ep")
    tp_index = lax.axis_index("tp")
    part_width = width // tp_count
    normed = rms_norm(tokens, mix_gain)
    drive = jnp.dot(normed, in_proj, preferred_element_type=jnp.float32).astype(jnp.bfloat16)
    reads, new_states = state_step(
        drive, states, decay_rate, frequency, log_step, b_real, b_imag, c_real, c_imag, skip_gain
    )
    partial_value = (
        jnp.dot(reads, out_proj, preferred_element_type=jnp.float32)
        .astype(jnp.bfloat16)
        .astype(jnp.float32)
    )
    mixed = lax.psum(partial_value.astype(jnp.bfloat16), "tp")
    resid = (tokens.astype(jnp.float32) + mixed.astype(jnp.float32)).astype(jnp.bfloat16)
    normed_two = rms_norm(resid, ffn_gain)
    own_cols = lax.dynamic_slice_in_dim(normed_two, tp_index * part_width, part_width, 1)
    hidden_width = dense_gate.shape[1]
    both_proj = jnp.concatenate([dense_gate, dense_up], axis=1)
    partial_both = jnp.dot(
        lax.all_gather(own_cols, "ep", axis=0, tiled=True),
        both_proj,
        preferred_element_type=jnp.float32,
    )
    summed_both = lax.psum(partial_both.astype(jnp.bfloat16), "tp").astype(jnp.float32)
    dense_hidden = (
        jax.nn.silu(summed_both[:, :hidden_width]) * summed_both[:, hidden_width:]
    ).astype(jnp.bfloat16)
    dense_term = lax.psum_scatter(
        jnp.dot(dense_hidden, dense_down, preferred_element_type=jnp.float32).astype(jnp.bfloat16),
        "ep",
        scatter_dimension=0,
        tiled=True,
    ).astype(jnp.float32)
    top_count = route_ids.shape[1]
    capacity = max(2, 2 * seq_count * top_count // ep_count)
    flat_ids = route_ids.reshape(-1)
    onehot = (flat_ids[:, None] == jnp.arange(ep_count, dtype=jnp.int32)[None, :]).astype(jnp.int32)
    rank = jnp.cumsum(onehot, axis=0) - onehot
    slot = jnp.sum(rank * onehot, axis=1)
    target = flat_ids * capacity + slot
    select = target[None, :] == jnp.arange(ep_count * capacity, dtype=jnp.int32)[:, None]
    select = jnp.any(select.reshape(ep_count * capacity, seq_count, top_count), axis=2).astype(
        jnp.bfloat16
    )
    send_rows = jnp.dot(select, normed_two, preferred_element_type=jnp.float32).astype(jnp.bfloat16)
    send_rows = send_rows.reshape(ep_count, capacity, width)
    send_part = lax.dynamic_slice_in_dim(send_rows, tp_index * part_width, part_width, 2)
    full_rows = lax.all_gather(
        lax.all_to_all(send_part, "ep", split_axis=0, concat_axis=0, tiled=True),
        "tp",
        axis=2,
        tiled=True,
    )
    answered = expert_rows(full_rows, expert_gate[0], expert_up[0], expert_down[0], part_width)
    returned = lax.all_to_all(answered, "ep", split_axis=0, concat_axis=0, tiled=True)
    picked_rows = returned.reshape(ep_count * capacity, part_width)[target]
    picked_rows = picked_rows.reshape(seq_count, top_count, part_width).astype(jnp.float32)
    route_weights = jax.nn.softmax(route_logits, axis=-1)
    routed = jnp.sum(route_weights[..., None] * picked_rows, axis=1)
    branch = jax.nn.sigmoid(jnp.dot(normed_two, branch_gate, preferred_element_type=jnp.float32))
    resid_cols = lax.dynamic_slice_in_dim(resid, tp_index * part_width, part_width, 1).astype(
        jnp.float32
    )
    output = (resid_cols + routed + branch[:, None] * dense_term).astype(jnp.bfloat16)
    return (output, new_states)


def solution(mesh):
    return jax.shard_map(
        shards,
        mesh=mesh,
        in_specs=(
            P("ep", None),
            P(),
            P(),
            P(None, "tp"),
            P("tp", None),
            P("tp", None),
            P("tp"),
            P("tp", None, None),
            P("tp", None, None),
            P("tp", None, None),
            P("tp", None, None),
            P("tp"),
            P(None, "ep", "tp"),
            P("tp", None),
            P("ep", None),
            P("ep", None),
            P("ep", None, "tp"),
            P("ep", None, "tp"),
            P("ep", "tp", None),
            P("tp", "ep"),
            P("tp", "ep"),
            P("ep", "tp"),
            P(),
        ),
        out_specs=(P("ep", "tp"), P(None, "ep", "tp")),
        check_vma=False,
    )
```

profile of v0, /device:TPU:0, one launch (start us, length us, event | category | flops | bytes accessed | tf_op | source)
XLA Modules:
  0.0 329.4 jit_solution(16527740815774029400)
XLA Ops:
  7.2 1.4 exp.20
  8.7 2.1 fusion.69
  10.7 1.2 copy.42
  11.9 2.2 copy.43
  14.4 2.8 convolution_convert_fusion.4
  18.9 1.9 fusion.26
  20.9 2.2 fusion.27
  23.1 1.5 fusion.70
  24.6 1.5 fusion.30
  26.2 1.4 convolution_convert_fusion.1
  27.9 37.6 %all-reduce.4.cloned.1.call-done = bf16[96,4096]{1,0:T(8,128)(2,1)} async-done(((bf16[96,4096]{1,0:T(8,128)(2,1)}), bf16[96,4096]{1,0:T(8,128)(2,1)}) %all-reduce.4.cloned.1.call-update) | async-done | bytes 786448 | tf_op jit(solution)/shard_map/psum | solution.py:113
  65.5 1.7 fusion.13
  72.6 1.0 convolution_convert_fusion
  73.7 30.8 %all_to_all.10 = bf16[8,48,1024]{2,1,0:T(8,128)(2,1)} all-to-all(bf16[8,48,1024]{2,1,0:T(8,128)(2,1)S(1)} %constant_dynamic-slice_fusion.1), channel_id=1, replica_groups=mesh['ep'=8,'tp'=4] {'ep'}, dimensions={0} | all-to-all | bytes 1572864 | tf_op jit(solution)/shard_map/all_to_all | solution.py:149
  104.6 14.9 %all-gather.5.cloned.1.call-done = bf16[768,1024]{1,0:T(8,128)(2,1)} async-done(((bf16[96,1024]{1,0:T(8,128)(2,1)}), bf16[768,1024]{1,0:T(8,128)(2,1)}) %all-gather.5.cloned.1.call-update) | async-done | bytes 1572880 | tf_op jit(solution)/shard_map/all_gather | solution.py:120
  119.5 6.4 %convolution_convert_fusion.2 = bf16[768,1536]{1,0:T(8,128)(2,1)} fusion(bf16[768,1024]{1,0:T(8,128)(2,1)} %all-gather.5.cloned.1.call-done, bf16[1024,768]{1,0:T(8,128)(2,1)} %param.43, bf16[1024,768]{1,0:T(8,128)(2,1)} %param.42), kind=kOutput, calls=%fused_computation.10 | convolution fusion | flops 2423390208 | bytes 7077888 | tf_op jit(solution)/shard_map/dot_general | solution.py:119
  126.1 22.0 %all-gather.3.cloned.1.call-done = bf16[8,48,4096]{2,1,0:T(8,128)(2,1)} async-done(((bf16[8,48,1024]{2,1,0:T(8,128)(2,1)}), bf16[8,48,4096]{2,1,0:T(8,128)(2,1)}) %all-gather.3.cloned.1.call-update) | async-done | bytes 3145744 | tf_op jit(solution)/shard_map/all_gather | solution.py:148
  148.1 7.4 %fusion.4 = f32[384,768]{1,0:T(8,128)} fusion(bf16[384,4096]{1,0:T(8,128)(2,1)} %bitcast.89, bf16[1,4096,768]{2,1,0:T(8,128)(2,1)} %param.39), kind=kOutput, calls=%fused_computation.5 | convolution fusion | flops 2415919104 | bytes 10616832 | tf_op jit(solution)/shard_map/dot_general | solution.py:59
  155.5 14.3 %fusion.6 = bf16[384,4096]{1,0:T(8,128)(2,1)} fusion(bf16[1,768,4096]{2,1,0:T(8,128)(2,1)} %param.41, bf16[384,4096]{1,0:T(8,128)(2,1)} %bitcast.90, bf16[1,4096,768]{2,1,0:T(8,128)(2,1)} %param.40, f32[384,768]{1,0:T(8,128)} %fusion.4), kind=kOutput, calls=%fused_computation.8 | convolution fusion | flops 4835180544 | bytes 20054016 | tf_op jit(solution)/shard_map/dot_general | solution.py:63
  169.9 36.2 %all-reduce.6.cloned.1.call-done = bf16[768,1536]{1,0:T(8,128)(2,1)} async-done(((bf16[768,1536]{1,0:T(8,128)(2,1)}), bf16[768,1536]{1,0:T(8,128)(2,1)}) %all-reduce.6.cloned.1.call-update) | async-done | bytes 2359312 | tf_op jit(solution)/shard_map/psum | solution.py:124
  206.0 2.4 convert_element_type.91
  208.5 2.6 convolution_convert_fusion.3
  211.1 35.2 %reduce-scatter.3.cloned.1.call-done = bf16[384,1024]{1,0:T(8,128)(2,1)} async-done(((bf16[384,4096]{1,0:T(8,128)(2,1)}), bf16[384,1024]{1,0:T(8,128)(2,1)}) %reduce-scatter.3.cloned.1.call-update) | async-done | bytes 786448 | tf_op jit(solution)/shard_map/reduce_scatter | solution.py:67
  246.2 5.5 %all-to-all-start.1 = ((bf16[8,48,1024]{2,1,0:T(8,128)(2,1)}), bf16[8,48,1024]{2,1,0:T(8,128)(2,1)S(1)}, u32[]{:S(2)}, u32[]{:S(2)}) async-start(bf16[8,48,1024]{2,1,0:T(8,128)(2,1)} %bitcast.86), calls=%async_computation.2 | async-start | bytes 1572864 | tf_op jit(solution)/shard_map/all_to_all | solution.py:155
  252.1 2.0 copy.50
  255.0 2.1 pad_maximum_fusion
  257.1 1.4 fusion.34
  258.5 22.2 %all-to-all-done.1 = bf16[8,48,1024]{2,1,0:T(8,128)(2,1)S(1)} async-done(((bf16[8,48,1024]{2,1,0:T(8,128)(2,1)}), bf16[8,48,1024]{2,1,0:T(8,128)(2,1)S(1)}, u32[]{:S(2)}, u32[]{:S(2)}) %all-to-all-start.1) | async-done | bytes 786464 | tf_op jit(solution)/shard_map/all_to_all | solution.py:155
  280.8 1.0 gather_fusion
  282.3 1.0 multiply_reduce_fusion
  283.3 37.4 %reduce-scatter.5.cloned.1.call-done = bf16[96,1024]{1,0:T(8,128)(2,1)} async-done(((bf16[768,1024]{1,0:T(8,128)(2,1)}), bf16[96,1024]{1,0:T(8,128)(2,1)}) %reduce-scatter.5.cloned.1.call-update) | async-done | bytes 196624 | tf_op jit(solution)/shard_map/reduce_scatter | solution.py:128
  320.7 1.8 add_convert_fusion
  (82 shorter events, 10.0 us)
Async XLA Ops:
  7.2 19.0 %copy-start = (bf16[256,4096]{1,0:T(8,128)(2,1)S(1)}, bf16[256,4096]{1,0:T(8,128)(2,1)}, u32[]{:S(2)}) copy-start(bf16[256,4096]{1,0:T(8,128)(2,1)} %param.36) | copy-start | bytes 6291460
  7.2 6.9 %copy-start.5 = (bf16[96,4096]{1,0:T(8,128)(2,1)S(1)}, bf16[96,4096]{1,0:T(8,128)(2,1)}, u32[]{:S(2)}) copy-start(bf16[96,4096]{1,0:T(8,128)(2,1)} %param.23) | copy-start | bytes 2359300
  7.2 58.3 %all-reduce.4.cloned.1.call-start = ((), (), s32[]{:S(2)}) async-start(), calls=%async_computation.4 | async-start | bytes 1572864 | tf_op jit(solution)/shard_map/psum | solution.py:113
  11.9 7.0 %copy-start.2 = (f32[1,96,1024]{1,2,0:T(8,128)}, f32[1,96,1024]{1,2,0:T(8,128)S(1)}, u32[]{:S(2)}) copy-start(f32[1,96,1024]{1,2,0:T(8,128)S(1)} %copy.42) | copy-start | bytes 1179652
  14.1 4.0 %copy-start.12 = (f32[16,64]{1,0:T(8,128)S(1)}, f32[16,64]{1,0:T(8,128)}, u32[]{:S(2)}) copy-start(f32[16,64]{1,0:T(8,128)} %param.28) | copy-start | bytes 12292
  14.1 4.0 %copy-start.13 = (f32[16,64]{1,0:T(8,128)S(1)}, f32[16,64]{1,0:T(8,128)}, u32[]{:S(2)}) copy-start(f32[16,64]{1,0:T(8,128)} %param.27) | copy-start | bytes 12292
  14.1 4.8 %copy-start.6 = (f32[16,64,16]{1,2,0:T(8,128)S(1)}, f32[16,64,16]{1,2,0:T(8,128)}, u32[]{:S(2)}) copy-start(f32[16,64,16]{1,2,0:T(8,128)} %param.31) | copy-start | bytes 196612
  17.1 3.7 %copy-start.7 = (f32[16,64,16]{1,2,0:T(8,128)S(1)}, f32[16,64,16]{1,2,0:T(8,128)}, u32[]{:S(2)}) copy-start(f32[16,64,16]{1,2,0:T(8,128)} %param.30) | copy-start | bytes 196612
  17.2 5.9 %copy-start.15 = (f32[256]{0:T(256)S(1)}, f32[256]{0:T(256)}, u32[]{:S(2)}) copy-start(f32[256]{0:T(256)} %param.34) | copy-start | bytes 3076
  20.9 6.7 %copy-start.1 = (f32[96,16,64]{0,2,1:T(8,128)}, f32[96,16,64]{0,2,1:T(8,128)S(1)}, u32[]{:S(2)}) copy-start(f32[96,16,64]{0,2,1:T(8,128)S(1)} %fusion.26) | copy-start | bytes 1179652
  26.1 1.5 copy-start.16
  27.5 40.6 %copy-start.8 = (f32[4096]{0:T(1024)S(1)}, f32[4096]{0:T(1024)}, u32[]{:S(2)}) copy-start(f32[4096]{0:T(1024)} %param.25) | copy-start | bytes 49156
  27.6 91.9 %all-gather.5.cloned.1.call-start = ((), (), s32[]{:S(2)}) async-start(), calls=%async_computation.7 | async-start | bytes 1769472 | tf_op jit(solution)/shard_map/all_gather | solution.py:120
  67.2 0.9 copy-start.4
  68.4 5.2 %copy-start.3 = (bf16[96,4096]{1,0:T(8,128)(2,1)}, bf16[96,4096]{1,0:T(8,128)(2,1)S(1)}, u32[]{:S(2)}) copy-start(bf16[96,4096]{1,0:T(8,128)(2,1)S(1)} %fusion.15) | copy-start | bytes 2359300
  69.2 78.9 %all-gather.3.cloned.1.call-start = ((), (), s32[]{:S(2)}) async-start(), calls=%async_computation.5 | async-start | bytes 3932160 | tf_op jit(solution)/shard_map/all_gather | solution.py:148
  70.3 0.6 copy-start.9
  104.6 101.5 %all-reduce.6.cloned.1.call-start = ((), (), s32[]{:S(2)}) async-start(), calls=%async_computation.8 | async-start | bytes 4718592 | tf_op jit(solution)/shard_map/psum | solution.py:124
  125.9 120.4 %reduce-scatter.3.cloned.1.call-start = ((), (), s32[]{:S(2)}) async-start(), calls=%async_computation.6 | async-start | bytes 3932160 | tf_op jit(solution)/shard_map/reduce_scatter | solution.py:67
  169.8 150.9 %reduce-scatter.5.cloned.1.call-start = ((), (), s32[]{:S(2)}) async-start(), calls=%async_computation.9 | async-start | bytes 1769472 | tf_op jit(solution)/shard_map/reduce_scatter | solution.py:128
  206.0 2.4 copy-start.17
  211.0 40.9 %copy-start.11 = (f32[96,2]{0,1:T(2,128)S(1)}, f32[96,2]{0,1:T(2,128)}, u32[]{:S(2)}) copy-start(f32[96,2]{0,1:T(2,128)} %param.38) | copy-start | bytes 2308
  211.0 41.0 %copy-start.14 = (bf16[4096]{0:T(1024)(128)(2,1)S(1)}, bf16[4096]{0:T(1024)(128)(2,1)}, u32[]{:S(2)}) copy-start(bf16[4096]{0:T(1024)(128)(2,1)} %param.45) | copy-start | bytes 24580
  211.1 43.9 %copy-start.10 = (s32[192]{0:T(256)S(1)}, s32[192]{0:T(256)}, u32[]{:S(2)}) copy-start(s32[192]{0:T(256)} %copy-done.9) | copy-start | bytes 2308
  246.2 34.5 %all-to-all-start.1 = ((bf16[8,48,1024]{2,1,0:T(8,128)(2,1)}), bf16[8,48,1024]{2,1,0:T(8,128)(2,1)S(1)}, u32[]{:S(2)}, u32[]{:S(2)}) async-start(bf16[8,48,1024]{2,1,0:T(8,128)(2,1)} %bitcast.86), calls=%async_computation.2 | async-start | bytes 1572864 | tf_op jit(solution)/shard_map/all_to_all | solution.py:155
Sparse Core Ops, SparseCore 0:
  27.7 37.7 all-reduce.3
  69.3 50.0 all-gather.4
  121.0 27.0 all-gather.2
  150.3 55.6 all-reduce.5
  208.4 37.7 reduce-scatter.2
  249.5 71.1 reduce-scatter.4
where the time goes:
time: 330 us; the launch traced here: 329 us
  waiting for transfers between devices  205 us (62%)
  matrix products  44.3 us (13%)
  blocking collectives  30.8 us (9%)
  local copies, waits for them, and re-layouts  16.2 us (5%)
  between operations  14.4 us (4%)
  other arithmetic  12.1 us (4%)
  starting transfers between devices  5.94 us (2%)
    psum x1, waiting for transfers between devices, shards(): mixed = lax.psum(partial_value.astype(jnp.bfloat16), 'tp')  37.6 us
    reduce_scatter x1, waiting for transfers between devices, shards(): lax.psum_scatter(jnp.dot(dense_hidden, dense_down, preferred_element_type...  37.4 us
    psum x1, waiting for transfers between devices, shards(): lax.psum(partial_both.astype(jnp.bfloat16), 'tp').astype(jnp.float32)  36.2 us
    reduce_scatter x1, waiting for transfers between devices, expert_rows(): lax.psum_scatter(partial_value.astype(jnp.bfloat16), 'tp', scatter_dimens...  35.2 us
    all_to_all x1, blocking collectives, shards(): lax.all_to_all(send_part, 'ep', split_axis=0, concat_axis=0, tiled=True)  30.8 us
    all_to_all x1, waiting for transfers between devices, shards(): lax.all_to_all(answered, 'ep', split_axis=0, concat_axis=0, tiled=True)  22.2 us
    all_gather x1, waiting for transfers between devices, shards(): lax.all_gather(lax.all_to_all(send_part, 'ep', split_axis=0, concat_axis=...  22 us
    all_gather x1, waiting for transfers between devices, shards(): lax.all_gather(own_cols, 'ep', axis=0, tiled=True)  14.9 us
  transfers between devices with their start and end apart: 7, of which 7 were waited for; matrix products, arithmetic and copies ran while one was open for 14% of the time, Pallas kernels for 0%

commit v1 on v0

v1 whole, which is shorter than its diff:
```python
import functools
import jax
import jax.numpy as jnp
from jax import lax
from jax.experimental import pallas as pl
from jax.experimental.pallas import tpu as pltpu
from jax.sharding import PartitionSpec as P

GROUP = 16
STATE = 64
MESH = pl.DeviceIdType.MESH


def fast_extent(axis, size):
    if axis == "tp":
        return 2
    extent = 1
    while (2 * extent) * (2 * extent) * 2 <= size:
        extent *= 2
    return extent


class Grid:
    def __init__(self, axis, size):
        self.axis, self.size = axis, size
        self.fast = fast_extent(axis, size)
        self.slow = size // self.fast
        self.me = lax.axis_index(axis)
        self.at_fast = self.me % self.fast
        self.at_slow = self.me // self.fast

    def index(self, slow_step, fast_step):
        slow_at = (self.at_slow + slow_step + self.slow) % self.slow
        fast_at = (self.at_fast + fast_step + self.fast) % self.fast
        return slow_at * self.fast + fast_at

    def peers(self):
        return [self.index(k, 0) for k in range(1, self.slow)] + [
            self.index(0, q) for q in range(1, self.fast)
        ]

    def greet(self):
        barrier = pltpu.get_barrier_semaphore()
        peers = self.peers()
        for peer in peers:
            pl.semaphore_signal(barrier, inc=1, device_id={self.axis: peer}, device_id_type=MESH)
        pl.semaphore_wait(barrier, len(peers))

    def copy(self, source, target, sent, landed, peer):
        return pltpu.make_async_remote_copy(
            src_ref=source,
            dst_ref=target,
            send_sem=sent,
            recv_sem=landed,
            device_id={self.axis: peer},
            device_id_type=MESH,
        )


def part_of(ref, owner, start, rows, width, cols):
    if cols:
        return ref.at[pl.ds(start, rows), pl.ds(pl.multiple_of(owner * width, 128), width)]
    return ref.at[owner, pl.ds(start, rows), :]


def gather_kernel(axis, size, pieces, cols, *refs):
    count = len(pieces)
    ins, outs = refs[:count], refs[count : 2 * count]
    slow_sent, slow_landed, fast_sent, fast_landed, own_sem = refs[2 * count :]
    grid = Grid(axis, size)
    spans = []
    for item, number in enumerate(pieces):
        rows = ins[item].shape[0] // number
        spans += [(item, j, j * rows, rows) for j in range(number)]

    def place(item, owner, start, rows):
        return part_of(outs[item], owner, start, rows, ins[item].shape[1], cols)

    grid.greet()
    pending = []
    for item, j, start, rows in spans:
        for k in range(1, grid.slow):
            copy = grid.copy(
                ins[item].at[pl.ds(start, rows), :],
                place(item, grid.me, start, rows),
                slow_sent.at[item, j, k - 1],
                slow_landed.at[item, j, k - 1],
                grid.index(k, 0),
            )
            copy.start()
            pending.append(copy)
    for item, j, start, rows in spans:
        for q in range(1, grid.fast):
            copy = grid.copy(
                ins[item].at[pl.ds(start, rows), :],
                place(item, grid.me, start, rows),
                fast_sent.at[item, j, 0, q - 1],
                fast_landed.at[item, j, 0, q - 1],
                grid.index(0, q),
            )
            copy.start()
            pending.append(copy)
    owns = []
    for item in range(count):
        own = pltpu.make_async_copy(
            ins[item], place(item, grid.me, 0, ins[item].shape[0]), own_sem.at[item]
        )
        own.start()
        owns.append(own)
    for item, j, start, rows in spans:
        for k in range(1, grid.slow):
            block = place(item, grid.index(-k, 0), start, rows)
            grid.copy(
                block,
                block,
                slow_sent.at[item, j, k - 1],
                slow_landed.at[item, j, k - 1],
                grid.index(-k, 0),
            ).wait_recv()
            for q in range(1, grid.fast):
                copy = grid.copy(
                    block,
                    block,
                    fast_sent.at[item, j, k, q - 1],
                    fast_landed.at[item, j, k, q - 1],
                    grid.index(0, q),
                )
                copy.start()
                pending.append(copy)
    for item, j, start, rows in spans:
        for k in range(grid.slow):
            for q in range(1, grid.fast):
                block = place(item, grid.index(-k, -q), start, rows)
                grid.copy(
                    block,
                    block,
                    fast_sent.at[item, j, k, q - 1],
                    fast_landed.at[item, j, k, q - 1],
                    grid.index(0, -q),
                ).wait_recv()
    for copy in pending:
        copy.wait_send()
    for own in owns:
        own.wait()


def all_gather(arrays, axis, size, pieces, cols, collective_id):
    shapes = []
    for array in arrays:
        rows, width = array.shape
        shape = (rows, size * width) if cols else (size, rows, width)
        shapes.append(jax.ShapeDtypeStruct(shape, array.dtype))
    fast = fast_extent(axis, size)
    slow = size // fast
    count, most = len(arrays), max(pieces)
    sems = [
        pltpu.SemaphoreType.DMA((count, most, slow - 1)),
        pltpu.SemaphoreType.DMA((count, most, slow - 1)),
        pltpu.SemaphoreType.DMA((count, most, slow, fast - 1)),
        pltpu.SemaphoreType.DMA((count, most, slow, fast - 1)),
        pltpu.SemaphoreType.DMA((count,)),
    ]
    return pl.pallas_call(
        functools.partial(gather_kernel, axis, size, pieces, cols),
        out_shape=shapes,
        in_specs=[pl.BlockSpec(memory_space=pltpu.VMEM)] * count,
        out_specs=[pl.BlockSpec(memory_space=pltpu.VMEM)] * count,
        scratch_shapes=sems,
        compiler_params=pltpu.CompilerParams(
            collective_id=collective_id, has_side_effects=True, vmem_limit_bytes=16 << 20
        ),
    )(*arrays)


def reduce_kernel(
    axis,
    size,
    number,
    cols,
    x_ref,
    o_ref,
    got_fast,
    mid,
    got_slow,
    total_ref,
    fast_sent,
    fast_landed,
    slow_sent,
    slow_landed,
):
    grid = Grid(axis, size)
    rows, width = o_ref.shape
    step = rows // number
    grid.greet()
    pending = []
    for k in range(1, grid.slow + 1):
        for j in range(number):
            for q in range(1, grid.fast):
                copy = grid.copy(
                    part_of(x_ref, grid.index(k, q), j * step, step, width, cols),
                    got_fast.at[q - 1, k - 1, pl.ds(j * step, step), :],
                    fast_sent.at[q - 1, k - 1, j],
                    fast_landed.at[q - 1, k - 1, j],
                    grid.index(0, q),
                )
                copy.start()
                pending.append(copy)
    for k in range(1, grid.slow + 1):
        for j in range(number):
            span = pl.ds(j * step, step)
            total = part_of(x_ref, grid.index(k, 0), j * step, step, width, cols)[...].astype(
                jnp.float32
            )
            for q in range(1, grid.fast):
                block = got_fast.at[q - 1, k - 1, span, :]
                grid.copy(
                    block,
                    block,
                    fast_sent.at[q - 1, k - 1, j],
                    fast_landed.at[q - 1, k - 1, j],
                    grid.index(0, -q),
                ).wait_recv()
                total = total + block[...].astype(jnp.float32)
            if k == grid.slow:
                total_ref[span, :] = total
            else:
                mid[k - 1, span, :] = total.astype(mid.dtype)
                copy = grid.copy(
                    mid.at[k - 1, span, :],
                    got_slow.at[k - 1, span, :],
                    slow_sent.at[k - 1, j],
                    slow_landed.at[k - 1, j],
                    grid.index(k, 0),
                )
                copy.start()
                pending.append(copy)
    for j in range(number):
        span = pl.ds(j * step, step)
        total = total_ref[span, :]
        for k in range(1, grid.slow):
            block = got_slow.at[k - 1, span, :]
            grid.copy(
                block,
                block,
                slow_sent.at[k - 1, j],
                slow_landed.at[k - 1, j],
                grid.index(-k, 0),
            ).wait_recv()
            total = total + block[...].astype(jnp.float32)
        o_ref[span, :] = total.astype(o_ref.dtype)
    for copy in pending:
        copy.wait_send()


def reduce_scatter(array, axis, size, number, cols, collective_id):
    if cols:
        rows, width = array.shape[0], array.shape[1] // size
    else:
        rows, width = array.shape[1:]
    fast = fast_extent(axis, size)
    slow = size // fast
    return pl.pallas_call(
        functools.partial(reduce_kernel, axis, size, number, cols),
        out_shape=jax.ShapeDtypeStruct((rows, width), array.dtype),
        in_specs=[pl.BlockSpec(memory_space=pltpu.VMEM)],
        out_specs=pl.BlockSpec(memory_space=pltpu.VMEM),
        scratch_shapes=[
            pltpu.VMEM((fast - 1, slow, rows, width), array.dtype),
            pltpu.VMEM((slow - 1, rows, width), array.dtype),
            pltpu.VMEM((slow - 1, rows, width), array.dtype),
            pltpu.VMEM((rows, width), jnp.float32),
            pltpu.SemaphoreType.DMA((fast - 1, slow, number)),
            pltpu.SemaphoreType.DMA((fast - 1, slow, number)),
            pltpu.SemaphoreType.DMA((slow - 1, number)),
            pltpu.SemaphoreType.DMA((slow - 1, number)),
        ],
        compiler_params=pltpu.CompilerParams(
            collective_id=collective_id, has_side_effects=True, vmem_limit_bytes=24 << 20
        ),
    )(array)

def rms_norm(values, gain):
    flt = values.astype(jnp.float32)
    scaled = flt * lax.rsqrt(jnp.mean(flt * flt, axis=-1, keepdims=True) + 1e-06)
    return (scaled * gain).astype(jnp.bfloat16)


def discretize(decay_rate, frequency, log_step, b_real, b_imag):
    step_size = jnp.exp(log_step)[:, None]
    lam_re = -decay_rate
    magnitude = jnp.exp(lam_re * step_size)
    abar_re = magnitude * jnp.cos(frequency * step_size)
    abar_im = magnitude * jnp.sin(frequency * step_size)
    denom = lam_re * lam_re + frequency * frequency
    fac_re = ((abar_re - 1.0) * lam_re + abar_im * frequency) / denom
    fac_im = (abar_im * lam_re - (abar_re - 1.0) * frequency) / denom
    bbar_re = fac_re[..., None] * b_real - fac_im[..., None] * b_imag
    bbar_im = fac_re[..., None] * b_imag + fac_im[..., None] * b_real
    return (abar_re, abar_im, bbar_re, bbar_im)


def state_step(
    drive, states, decay_rate, frequency, log_step, b_real, b_imag, c_real, c_imag, skip_gain
):
    count = drive.shape[0]
    groups = decay_rate.shape[0]
    abar_re, abar_im, bbar_re, bbar_im = discretize(decay_rate, frequency, log_step, b_real, b_imag)
    grouped = drive.astype(jnp.float32).reshape(count, groups, GROUP)
    old_re = states[0].reshape(count, groups, STATE)
    old_im = states[1].reshape(count, groups, STATE)
    high = lax.Precision.HIGHEST
    push_re = jnp.einsum("ngh,gph->ngp", grouped, bbar_re, precision=high)
    push_im = jnp.einsum("ngh,gph->ngp", grouped, bbar_im, precision=high)
    new_re = abar_re * old_re - abar_im * old_im + push_re
    new_im = abar_re * old_im + abar_im * old_re + push_im
    readout = (
        jnp.einsum("ngp,ghp->ngh", new_re, c_real, precision=high)
        - jnp.einsum("ngp,ghp->ngh", new_im, c_imag, precision=high)
        + skip_gain.reshape(groups, GROUP) * grouped
    )
    reads = jax.nn.gelu(readout.reshape(count, groups * GROUP)).astype(jnp.bfloat16)
    fresh = jnp.stack(
        [new_re.reshape(count, groups * STATE), new_im.reshape(count, groups * STATE)]
    )
    return (reads, fresh)


def shards(
    tokens,
    mix_gain,
    ffn_gain,
    in_proj,
    decay_rate,
    frequency,
    log_step,
    b_real,
    b_imag,
    c_real,
    c_imag,
    skip_gain,
    states,
    out_proj,
    route_ids,
    route_logits,
    expert_gate,
    expert_up,
    expert_down,
    dense_gate,
    dense_up,
    dense_down,
    branch_gate,
):
    seq_count, width = tokens.shape
    tp_count = lax.axis_size("tp")
    ep_count = lax.axis_size("ep")
    tp_index = lax.axis_index("tp")
    part_width = width // tp_count
    normed = rms_norm(tokens, mix_gain)
    drive = jnp.dot(normed, in_proj, preferred_element_type=jnp.float32).astype(jnp.bfloat16)
    reads, new_states = state_step(
        drive, states, decay_rate, frequency, log_step, b_real, b_imag, c_real, c_imag, skip_gain
    )
    partial_value = (
        jnp.dot(reads, out_proj, preferred_element_type=jnp.float32)
        .astype(jnp.bfloat16)
        .astype(jnp.float32)
    )
    mixed_cols = reduce_scatter(partial_value.astype(jnp.bfloat16), "tp", tp_count, 2, True, 0)
    (mixed,) = all_gather([mixed_cols], "tp", tp_count, [2], True, 1)
    resid = (tokens.astype(jnp.float32) + mixed.astype(jnp.float32)).astype(jnp.bfloat16)
    normed_two = rms_norm(resid, ffn_gain)
    own_cols = lax.dynamic_slice_in_dim(normed_two, tp_index * part_width, part_width, 1)
    branch = jax.nn.sigmoid(jnp.dot(normed_two, branch_gate, preferred_element_type=jnp.float32))
    route_weights = jax.nn.softmax(route_logits, axis=-1)
    top_count = route_ids.shape[1]
    side = jnp.concatenate(
        [route_ids.astype(jnp.float32), route_weights, branch[:, None]], axis=1
    )
    side = jnp.pad(side, ((0, 0), (0, 128 - side.shape[1])))
    every_cols, every_side = all_gather([own_cols, side], "ep", ep_count, [1, 1], False, 2)
    total_count = ep_count * seq_count
    every_cols = every_cols.reshape(total_count, part_width)
    every_side = every_side.reshape(total_count, 128)
    every_ids = every_side[:, :top_count]
    every_weights = every_side[:, top_count : 2 * top_count]
    every_branch = every_side[:, 2 * top_count]
    mine = every_ids == lax.axis_index("ep").astype(jnp.float32)
    taken = jnp.any(mine, axis=1)
    own_weight = jnp.sum(jnp.where(mine, every_weights, 0.0), axis=1)
    order = jnp.cumsum(taken.astype(jnp.int32)) - 1
    room = ep_count * max(2, 2 * seq_count * top_count // ep_count)
    slots = jnp.arange(room, dtype=jnp.int32)
    select = (order[None, :] == slots[:, None]) & taken[None, :]
    row_weight = jnp.sum(jnp.where(select, own_weight[None, :], 0.0), axis=1)
    select = select.astype(jnp.bfloat16)
    expert_in = jnp.dot(select, every_cols, preferred_element_type=jnp.float32).astype(jnp.bfloat16)
    (full_rows,) = all_gather([expert_in], "tp", tp_count, [4], True, 3)
    hidden_width = dense_gate.shape[1]
    gate_part = jnp.dot(every_cols, dense_gate, preferred_element_type=jnp.float32)
    up_part = jnp.dot(every_cols, dense_up, preferred_element_type=jnp.float32)
    both = jnp.concatenate([gate_part.astype(jnp.bfloat16), up_part.astype(jnp.bfloat16)], axis=1)
    both = both.reshape(tp_count, total_count // tp_count, 2 * hidden_width)
    summed = reduce_scatter(both, "tp", tp_count, 4, False, 4).astype(jnp.float32)
    own_hidden = (
        jax.nn.silu(summed[:, :hidden_width]) * summed[:, hidden_width:]
    ).astype(jnp.bfloat16)
    (dense_hidden,) = all_gather([own_hidden], "tp", tp_count, [2], False, 5)
    dense_hidden = dense_hidden.reshape(total_count, hidden_width)
    gate_val = jnp.dot(full_rows, expert_gate[0], preferred_element_type=jnp.float32)
    up_val = jnp.dot(full_rows, expert_up[0], preferred_element_type=jnp.float32)
    hidden = (jax.nn.silu(gate_val) * up_val).astype(jnp.bfloat16)
    expert_part = jnp.dot(hidden, expert_down[0], preferred_element_type=jnp.float32)
    expert_cols = reduce_scatter(expert_part.astype(jnp.bfloat16), "tp", tp_count, 4, True, 6)
    weighted = (expert_cols.astype(jnp.float32) * row_weight[:, None]).astype(jnp.bfloat16)
    routed_part = lax.dot_general(
        select, weighted, (((0,), (0,)), ((), ())), preferred_element_type=jnp.float32
    )
    dense_part = jnp.dot(dense_hidden, dense_down, preferred_element_type=jnp.float32)
    share = (routed_part + every_branch[:, None] * dense_part).astype(jnp.bfloat16)
    share = share.reshape(ep_count, seq_count, part_width)
    gathered = reduce_scatter(share, "ep", ep_count, 1, False, 7)
    resid_cols = lax.dynamic_slice_in_dim(resid, tp_index * part_width, part_width, 1)
    output = (resid_cols.astype(jnp.float32) + gathered.astype(jnp.float32)).astype(jnp.bfloat16)
    return (output, new_states)


def solution(mesh):
    return jax.shard_map(
        shards,
        mesh=mesh,
        in_specs=(
            P("ep", None),
            P(),
            P(),
            P(None, "tp"),
            P("tp", None),
            P("tp", None),
            P("tp"),
            P("tp", None, None),
            P("tp", None, None),
            P("tp", None, None),
            P("tp", None, None),
            P("tp"),
            P(None, "ep", "tp"),
            P("tp", None),
            P("ep", None),
            P("ep", None),
            P("ep", None, "tp"),
            P("ep", None, "tp"),
            P("ep", "tp", None),
            P("tp", "ep"),
            P("tp", "ep"),
            P("ep", "tp"),
            P(),
        ),
        out_specs=(P("ep", "tp"), P(None, "ep", "tp")),
        check_vma=False,
    )
```

time: 330 us -> 220 us (0.67)
  waiting for transfers between devices: 205 us -> 0 us
  Pallas kernels: 0 us -> 150 us
  blocking collectives: 30.8 us -> 0 us
  between operations: 14.4 us -> 1.09 us
  matrix products: 44.3 us -> 37.6 us
  starting transfers between devices: 5.94 us -> 0 us
    pallas_call x0 -> x8, Pallas kernels: none -> 150 us  [the longest x4 78 us: reduce_scatter(): pl.pallas_call(functools.partial(reduce_kernel, axis, size, number, cols)...]
    psum x2 -> x0, waiting for transfers between devices: 73.8 us -> none  [the longest x1 37.6 us: shards(): mixed = lax.psum(partial_value.astype(jnp.bfloat16), 'tp')]
    reduce_scatter x2 -> x0, waiting for transfers between devices: 72.5 us -> none  [the longest x1 37.4 us: shards(): lax.psum_scatter(jnp.dot(dense_hidden, dense_down, preferred_element_type...]
    all_gather x2 -> x0, waiting for transfers between devices: 36.9 us -> none  [the longest x1 22 us: shards(): lax.all_gather(lax.all_to_all(send_part, 'ep', split_axis=0, concat_axis=...]
    all_to_all x1 -> x0, blocking collectives: 30.8 us -> none  [shards(): lax.all_to_all(send_part, 'ep', split_axis=0, concat_axis=0, tiled=True)]
    all_to_all x1 -> x0, waiting for transfers between devices: 22.2 us -> none  [shards(): lax.all_to_all(answered, 'ep', split_axis=0, concat_axis=0, tiled=True)]
    unnamed x38 -> x45, local copies, waits for them, and re-layouts: 1.64 us -> 8.03 us
    all_to_all x1 -> x0, starting transfers between devices: 5.51 us -> none  [shards(): lax.all_to_all(answered, 'ep', split_axis=0, concat_axis=0, tiled=True)]
  transfers between devices with their start and end apart: 7 -> 0, of which waited for: 7 -> 0; matrix products, arithmetic and copies ran while one was open for 14% -> 0% of each run, Pallas kernels for 0% -> 0%
where the time goes in v1:
time: 220 us; the launch traced here: 219 us
  Pallas kernels  150 us (68%)
  matrix products  37.6 us (17%)
  local copies, waits for them, and re-layouts  17.2 us (8%)
  other arithmetic  13.3 us (6%)
    pallas_call x4, Pallas kernels, reduce_scatter(): pl.pallas_call(functools.partial(reduce_kernel, axis, size, number, cols)...  78 us
    pallas_call x4, Pallas kernels, all_gather(): pl.pallas_call(functools.partial(gather_kernel, axis, size, pieces, cols)...  72.4 us
    dot_general x1, matrix products, shards(): jnp.dot(hidden, expert_down[0], preferred_element_type=jnp.float32)  14.2 us
    unnamed x45, local copies, waits for them, and re-layouts  8.03 us
    dot_general x1, matrix products, shards(): jnp.dot(full_rows, expert_gate[0], preferred_element_type=jnp.float32)  6.45 us

profile of v1, /device:TPU:0, one launch (start us, length us, event | category | flops | bytes accessed | tf_op | source)
XLA Modules:
  0.0 219.5 jit_solution(16538152958855114211)
XLA Ops:
  0.7 0.8 reduce_max.9
  2.2 1.3 fusion.66
  4.1 1.4 fusion.12
  5.5 1.2 convert_element_type.96
  9.1 2.4 %convolution_convert_fusion.4 = bf16[96,256]{1,0:T(8,128)(2,1)S(1)} fusion(bf16[4096,256]{1,0:T(8,128)(2,1)} %param.26, bf16[96,4096]{1,0:T(8,128)(2,1)} %param.23, f32[4096]{0:T(1024)} %param.24, f32[96]{0:T(128)S(1)} %add_rsqrt_fusion.1), kind=kOutput, calls=%fused_computation.39 | convolution fusion | flops 202924032 | bytes 2949504 | tf_op jit(solution)/shard_map/dot_general | solution.py:359
  11.6 1.2 fusion.70
  13.0 1.0 copy.61
  14.0 2.0 fusion.22
  16.1 1.9 fusion.23
  20.2 0.9 pad_maximum_fusion.1
  21.6 9.6 %shard_map.230.refs_0_ = bf16[96,1024]{1,0:T(8,128)(2,1)S(1)} custom-call(bf16[96,4096]{1,0:T(8,128)(2,1)S(1)} %convolution_convert_fusion.x_ref), custom_call_target="tpu_custom_call" | custom-call | tf_op jit(solution)/shard_map/pallas_call | solution.py:262
  31.2 8.2 %shard_map.231 = bf16[96,4096]{1,0:T(8,128)(2,1)S(1)} custom-call(bf16[96,1024]{1,0:T(8,128)(2,1)S(1)} %shard_map.230.refs_0_), custom_call_target="tpu_custom_call" | custom-call | tf_op jit(solution)/shard_map/pallas_call | solution.py:163
  41.2 32.9 %shard_map.232 = (bf16[8,96,1024]{2,1,0:T(8,128)(2,1)S(1)}, f32[8,96,128]{2,1,0:T(8,128)S(1)}) custom-call(bf16[96,1024]{1,0:T(8,128)(2,1)S(1)} %constant_dynamic-slice_fusion.refs_0_, f32[96,128]{1,0:T(8,128)S(1)} %pad.4.refs_1_), custom_call_target="tpu_custom_call" | custom-call | tf_op jit(solution)/shard_map/pallas_call | solution.py:163
  74.1 1.1 copy-done.5
  76.9 3.2 %convolution_convert_fusion.3.refs_0_ = bf16[384,1024]{1,0:T(8,128)(2,1)} fusion(bf16[768,1024]{1,0:T(8,128)(2,1)} %bitcast.84, s32[768]{0:T(1024)S(1)} %add_bitcast_fusion, pred[768]{0:T(1024)(128)(4,1)S(1)} %reduce_or.9), kind=kOutput, calls=%fused_computation.26 | convolution fusion | flops 604962816 | bytes 2363136 | tf_op jit(solution)/shard_map/dot_general | solution.py:396
  80.1 1.5 convolution_convert_fusion.1
  81.7 1.5 convolution_convert_fusion.2
  83.2 1.6 pad_maximum_fusion
  84.7 4.3 %copy.65 = bf16[768,1536]{1,0:T(8,128)(2,1)} copy(bf16[768,1536]{0,1:T(8,128)(2,1)} %pad_maximum_fusion) | data formatting | bytes 4718592 | tf_op jit(solution)/shard_map/concatenate | solution.py:401
  89.0 1.7 copy-done.1
  90.7 16.9 %shard_map.235 = bf16[192,1536]{1,0:T(8,128)(2,1)S(1)} custom-call(bf16[4,192,1536]{2,1,0:T(8,128)(2,1)S(1)} %bitcast.79), custom_call_target="tpu_custom_call" | custom-call | tf_op jit(solution)/shard_map/pallas_call | solution.py:262
  107.9 10.2 %shard_map.236 = bf16[4,192,768]{2,1,0:T(8,128)(2,1)S(1)} custom-call(bf16[192,768]{1,0:T(8,128)(2,1)S(1)} %fusion.41.refs_0_), custom_call_target="tpu_custom_call" | custom-call | tf_op jit(solution)/shard_map/pallas_call | solution.py:163
  118.1 21.2 %shard_map.233 = bf16[384,4096]{1,0:T(8,128)(2,1)S(1)} custom-call(bf16[384,1024]{1,0:T(8,128)(2,1)S(1)} %copy-done.4), custom_call_target="tpu_custom_call" | custom-call | tf_op jit(solution)/shard_map/pallas_call | solution.py:163
  139.3 1.7 copy-done.2
  140.9 6.4 %fusion.4 = f32[384,768]{1,0:T(8,128)} fusion(bf16[384,4096]{1,0:T(8,128)(2,1)S(1)} %shard_map.233, bf16[1,4096,768]{2,1,0:T(8,128)(2,1)} %param.39), kind=kOutput, calls=%fused_computation.4 | convolution fusion | flops 2415919104 | bytes 10616832 | tf_op jit(solution)/shard_map/dot_general | solution.py:409
  147.4 14.2 %fusion.6.x_ref = bf16[384,4096]{1,0:T(8,128)(2,1)} fusion(bf16[1,768,4096]{2,1,0:T(8,128)(2,1)} %param.41, bf16[384,4096]{1,0:T(8,128)(2,1)} %copy-done.2, bf16[1,4096,768]{2,1,0:T(8,128)(2,1)} %param.40, f32[384,768]{1,0:T(8,128)} %fusion.4), kind=kOutput, calls=%fused_computation.6 | convolution fusion | flops 4835180544 | bytes 20054016 | tf_op jit(solution)/shard_map/dot_general | solution.py:412
  161.6 1.9 copy-done.3
  163.5 21.5 %shard_map.234 = bf16[384,1024]{1,0:T(8,128)(2,1)S(1)} custom-call(bf16[384,4096]{1,0:T(8,128)(2,1)S(1)} %copy-done.3), custom_call_target="tpu_custom_call" | custom-call | tf_op jit(solution)/shard_map/pallas_call | solution.py:262
  185.0 1.1 fusion.25
  186.4 1.4 add_convert_fusion
  187.8 30.0 %shard_map.237 = bf16[96,1024]{1,0:T(8,128)(2,1)S(1)} custom-call(bf16[8,96,1024]{2,1,0:T(8,128)(2,1)S(1)} %bitcast.82), custom_call_target="tpu_custom_call" | custom-call | tf_op jit(solution)/shard_map/pallas_call | solution.py:262
  217.8 1.7 add_convert_fusion.1
  (74 shorter events, 10.7 us)
Async XLA Ops:
  0.6 20.5 %copy-start = (bf16[256,4096]{1,0:T(8,128)(2,1)S(1)}, bf16[256,4096]{1,0:T(8,128)(2,1)}, u32[]{:S(2)}) copy-start(bf16[256,4096]{1,0:T(8,128)(2,1)} %param.36) | copy-start | bytes 6291460
  13.0 1.0 copy-start.7
  13.0 3.1 %copy-start.11 = (f32[16,64,16]{1,2,0:T(8,128)S(1)}, f32[16,64,16]{1,2,0:T(8,128)}, u32[]{:S(2)}) copy-start(f32[16,64,16]{1,2,0:T(8,128)} %param.31) | copy-start | bytes 196612
  13.0 3.1 %copy-start.12 = (f32[16,64,16]{1,2,0:T(8,128)S(1)}, f32[16,64,16]{1,2,0:T(8,128)}, u32[]{:S(2)}) copy-start(f32[16,64,16]{1,2,0:T(8,128)} %param.30) | copy-start | bytes 196612
  14.0 2.1 copy-start.8
  14.0 3.9 %copy-start.15 = (f32[16,16,64]{2,1,0:T(8,128)S(1)}, f32[16,16,64]{2,1,0:T(8,128)}, u32[]{:S(2)}) copy-start(f32[16,16,64]{2,1,0:T(8,128)} %param.32) | copy-start | bytes 196612
  16.1 2.5 %copy-start.14 = (f32[16,16,64]{2,1,0:T(8,128)S(1)}, f32[16,16,64]{2,1,0:T(8,128)}, u32[]{:S(2)}) copy-start(f32[16,16,64]{2,1,0:T(8,128)} %param.33) | copy-start | bytes 196612
  20.0 1.1 copy-start.13
  21.6 17.8 %copy-start.10 = (bf16[96,4096]{1,0:T(8,128)(2,1)S(1)}, bf16[96,4096]{1,0:T(8,128)(2,1)}, u32[]{:S(2)}) copy-start(bf16[96,4096]{1,0:T(8,128)(2,1)} %param.23) | copy-start | bytes 2359300
  31.2 8.6 %copy-start.16 = (f32[4096]{0:T(1024)S(1)}, f32[4096]{0:T(1024)}, u32[]{:S(2)}) copy-start(f32[4096]{0:T(1024)} %param.25) | copy-start | bytes 49156
  39.8 0.9 copy-start.9
  39.8 1.2 copy-start.17
  39.8 1.2 copy-start.18
  74.0 1.2 copy-start.5
  76.9 3.3 %copy-start.6 = (bf16[8,96,1024]{2,1,0:T(8,128)(2,1)S(1)}, bf16[8,96,1024]{2,1,0:T(8,128)(2,1)}, u32[]{:S(2)}) copy-start(bf16[8,96,1024]{2,1,0:T(8,128)(2,1)} %copy-done.5) | copy-start | bytes 4718596
  76.9 3.3 %copy-start.19 = (bf16[1024,768]{1,0:T(8,128)(2,1)S(1)}, bf16[1024,768]{1,0:T(8,128)(2,1)}, u32[]{:S(2)}) copy-start(bf16[1024,768]{1,0:T(8,128)(2,1)} %param.43) | copy-start | bytes 4718596
  80.1 1.5 copy-start.20
  89.0 1.7 copy-start.1
  107.7 10.4 %copy-start.4 = (bf16[384,1024]{1,0:T(8,128)(2,1)S(1)}, bf16[384,1024]{1,0:T(8,128)(2,1)}, u32[]{:S(2)}) copy-start(bf16[384,1024]{1,0:T(8,128)(2,1)} %convolution_convert_fusion.3.refs_0_) | copy-start | bytes 2359300
  139.3 1.7 copy-start.2
  161.6 1.9 copy-start.3
  185.0 1.4 copy-start.21

commit v2 on v1

--- a/solution.py
+++ b/solution.py
@@ -279,6 +279,315 @@
         ),
     )(array)
 
+class Gather:
+    def __init__(self, grid, source, target, number, cols, sems):
+        self.grid, self.source, self.target, self.cols = grid, source, target, cols
+        self.slow_sent, self.slow_landed, self.fast_sent, self.fast_landed, self.own_sem = sems
+        self.rows, self.width = source.shape
+        self.step = self.rows // number
+        self.number = number
+        self.pending = []
+
+    def place(self, owner, j):
+        return part_of(self.target, owner, j * self.step, self.step, self.width, self.cols)
+
+    def slow_copy(self, source, target, j, k, peer):
+        return self.grid.copy(
+            source, target, self.slow_sent.at[j, k - 1], self.slow_landed.at[j, k - 1], peer
+        )
+
+    def fast_copy(self, source, target, j, k, q, peer):
+        return self.grid.copy(
+            source, target, self.fast_sent.at[j, k, q - 1], self.fast_landed.at[j, k, q - 1], peer
+        )
+
+    def launch(self, copy):
+        copy.start()
+        self.pending.append(copy)
+
+    def start(self):
+        grid = self.grid
+        for j in range(self.number):
+            piece = self.source.at[pl.ds(j * self.step, self.step), :]
+            spot = self.place(grid.me, j)
+            for k in range(1, grid.slow):
+                self.launch(self.slow_copy(piece, spot, j, k, grid.index(k, 0)))
+        for j in range(self.number):
+            piece = self.source.at[pl.ds(j * self.step, self.step), :]
+            spot = self.place(grid.me, j)
+            for q in range(1, grid.fast):
+                self.launch(self.fast_copy(piece, spot, j, 0, q, grid.index(0, q)))
+        self.own = pltpu.make_async_copy(
+            self.source,
+            part_of(self.target, grid.me, 0, self.rows, self.width, self.cols),
+            self.own_sem,
+        )
+        self.own.start()
+
+    def relay(self):
+        grid = self.grid
+        for j in range(self.number):
+            for k in range(1, grid.slow):
+                spot = self.place(grid.index(-k, 0), j)
+                self.slow_copy(spot, spot, j, k, grid.index(-k, 0)).wait_recv()
+                for q in range(1, grid.fast):
+                    self.launch(self.fast_copy(spot, spot, j, k, q, grid.index(0, q)))
+
+    def arrive(self):
+        grid = self.grid
+        for j in range(self.number):
+            for k in range(grid.slow):
+                for q in range(1, grid.fast):
+                    spot = self.place(grid.index(-k, -q), j)
+                    self.fast_copy(spot, spot, j, k, q, grid.index(0, -q)).wait_recv()
+        self.own.wait()
+
+    def finish(self):
+        for copy in self.pending:
+            copy.wait_send()
+
+
+def gather_sems(grid_fast, grid_slow, number):
+    return [
+        pltpu.SemaphoreType.DMA((number, grid_slow - 1)),
+        pltpu.SemaphoreType.DMA((number, grid_slow - 1)),
+        pltpu.SemaphoreType.DMA((number, grid_slow, grid_fast - 1)),
+        pltpu.SemaphoreType.DMA((number, grid_slow, grid_fast - 1)),
+        pltpu.SemaphoreType.DMA,
+    ]
+
+
+class Reduce:
+    def __init__(self, grid, source, number, cols, scratch):
+        self.grid, self.source, self.cols, self.number = grid, source, cols, number
+        self.got_fast, self.mid, self.got_slow, self.total = scratch[:4]
+        self.fast_sent, self.fast_landed, self.slow_sent, self.slow_landed = scratch[4:]
+        rows, self.width = self.total.shape
+        self.step = rows // number
+        self.pending = []
+
+    def part(self, dest, j):
+        return part_of(self.source, dest, j * self.step, self.step, self.width, self.cols)
+
+    def span(self, j):
+        return pl.ds(j * self.step, self.step)
+
+    def fast_copy(self, source, k, j, q, peer):
+        return self.grid.copy(
+            source,
+            self.got_fast.at[q - 1, k - 1, self.span(j), :],
+            self.fast_sent.at[q - 1, k - 1, j],
+            self.fast_landed.at[q - 1, k - 1, j],
+            peer,
+        )
+
+    def slow_copy(self, k, j, peer):
+        return self.grid.copy(
+            self.mid.at[k - 1, self.span(j), :],
+            self.got_slow.at[k - 1, self.span(j), :],
+            self.slow_sent.at[k - 1, j],
+            self.slow_landed.at[k - 1, j],
+            peer,
+        )
+
+    def push(self):
+        grid = self.grid
+        for k in range(1, grid.slow + 1):
+            for j in range(self.number):
+                for q in range(1, grid.fast):
+                    copy = self.fast_copy(
+                        self.part(grid.index(k, q), j), k, j, q, grid.index(0, q)
+                    )
+                    copy.start()
+                    self.pending.append(copy)
+
+    def relay(self):
+        grid = self.grid
+        for k in range(1, grid.slow + 1):
+            for j in range(self.number):
+                value = self.part(grid.index(k, 0), j)[...].astype(jnp.float32)
+                for q in range(1, grid.fast):
+                    block = self.got_fast.at[q - 1, k - 1, self.span(j), :]
+                    self.fast_copy(block, k, j, q, grid.index(0, -q)).wait_recv()
+                    value = value + block[...].astype(jnp.float32)
+                if k == grid.slow:
+                    self.total[self.span(j), :] = value
+                else:
+                    self.mid[k - 1, self.span(j), :] = value.astype(self.mid.dtype)
+                    copy = self.slow_copy(k, j, grid.index(k, 0))
+                    copy.start()
+                    self.pending.append(copy)
+
+    def collect(self, emit):
+        grid = self.grid
+        for j in range(self.number):
+            value = self.total[self.span(j), :]
+            for k in range(1, grid.slow):
+                self.slow_copy(k, j, grid.index(-k, 0)).wait_recv()
+                value = value + self.got_slow[k - 1, self.span(j), :].astype(jnp.float32)
+            emit(self.span(j), value)
+
+    def finish(self):
+        for copy in self.pending:
+            copy.wait_send()
+
+
+def reduce_scratch(fast, slow, rows, width, number):
+    return [
+        pltpu.VMEM((fast - 1, slow, rows, width), jnp.bfloat16),
+        pltpu.VMEM((slow - 1, rows, width), jnp.bfloat16),
+        pltpu.VMEM((slow - 1, rows, width), jnp.bfloat16),
+        pltpu.VMEM((rows, width), jnp.float32),
+        pltpu.SemaphoreType.DMA((fast - 1, slow, number)),
+        pltpu.SemaphoreType.DMA((fast - 1, slow, number)),
+        pltpu.SemaphoreType.DMA((slow - 1, number)),
+        pltpu.SemaphoreType.DMA((slow - 1, number)),
+    ]
+
+
+def tile_of(extent):
+    for tile in (256, 128):
+        if extent % tile == 0:
+            return tile
+    return extent
+
+
+def branches_kernel(
+    axis,
+    size,
+    rows_ref,
+    cols_ref,
+    dense_gate,
+    dense_up,
+    gate_hbm,
+    up_hbm,
+    down_hbm,
+    dense_out,
+    expert_out,
+    full,
+    gate,
+    up,
+    down,
+    both,
+    own_hidden,
+    hidden,
+    part,
+    weight_sems,
+    *rest,
+):
+    grid = Grid(axis, size)
+    rows_gather = Gather(grid, rows_ref, full, ROW_PIECES, True, rest[:5])
+    hidden_gather = Gather(grid, own_hidden, dense_out, 2, False, rest[5:10])
+    dense_sum = Reduce(grid, both, 4, False, rest[10:18])
+    expert_sum = Reduce(grid, part, 4, True, rest[18:26])
+    loads = []
+    for item, (source, target) in enumerate(((gate_hbm, gate), (up_hbm, up), (down_hbm, down))):
+        load = pltpu.make_async_copy(source, target, weight_sems.at[item])
+        load.start()
+        loads.append(load)
+    grid.greet()
+    rows_gather.start()
+    share, double = both.shape[1:]
+    width = double // 2
+
+    @pl.loop(0, size)
+    def _(dest):
+        start = pl.multiple_of(dest * share, 16)
+        block = cols_ref[pl.ds(start, share), :]
+        both[dest, :, :width] = jnp.dot(
+            block, dense_gate[...], preferred_element_type=jnp.float32
+        ).astype(jnp.bfloat16)
+        both[dest, :, width:] = jnp.dot(
+            block, dense_up[...], preferred_element_type=jnp.float32
+        ).astype(jnp.bfloat16)
+
+    dense_sum.push()
+    dense_sum.relay()
+    rows_gather.relay()
+    rows_gather.arrive()
+    loads[0].wait()
+    loads[1].wait()
+    inner = hidden.shape[1]
+    tile = tile_of(inner)
+
+    @pl.loop(0, inner // tile)
+    def _(step):
+        span = pl.ds(pl.multiple_of(step * tile, 128), tile)
+        gate_val = jnp.dot(full[...], gate[:, span], preferred_element_type=jnp.float32)
+        up_val = jnp.dot(full[...], up[:, span], preferred_element_type=jnp.float32)
+        hidden[:, span] = (jax.nn.silu(gate_val) * up_val).astype(jnp.bfloat16)
+
+    def emit_hidden(span, value):
+        own_hidden[span, :] = (jax.nn.silu(value[:, :width]) * value[:, width:]).astype(
+            jnp.bfloat16
+        )
+
+    dense_sum.collect(emit_hidden)
+    loads[2].wait()
+    hidden_gather.start()
+    wide = 2 * tile_of(part.shape[1])
+
+    @pl.loop(0, part.shape[1] // wide)
+    def _(step):
+        span = pl.ds(pl.multiple_of(step * wide, 128), wide)
+        part[:, span] = jnp.dot(
+            hidden[...], down[:, span], preferred_element_type=jnp.float32
+        ).astype(jnp.bfloat16)
+
+    expert_sum.push()
+    expert_sum.relay()
+    hidden_gather.relay()
+    hidden_gather.arrive()
+
+    def emit_expert(span, value):
+        expert_out[span, :] = value.astype(expert_out.dtype)
+
+    expert_sum.collect(emit_expert)
+    for phase in (rows_gather, hidden_gather, dense_sum, expert_sum):
+        phase.finish()
+
+
+ROW_PIECES = 4
+
+
+def branches(rows, every_cols, dense_gate, dense_up, gate, up, down, axis, size, collective_id):
+    room, width = rows.shape
+    total, hidden_width = every_cols.shape[0], dense_gate.shape[1]
+    share, inner = total // size, gate.shape[1]
+    fast = fast_extent(axis, size)
+    slow = size // fast
+    whole = pl.BlockSpec(memory_space=pltpu.VMEM)
+    far = pl.BlockSpec(memory_space=pl.ANY)
+    bf16 = jnp.bfloat16
+    return pl.pallas_call(
+        functools.partial(branches_kernel, axis, size),
+        out_shape=(
+            jax.ShapeDtypeStruct((size, share, hidden_width), bf16),
+            jax.ShapeDtypeStruct((room, width), bf16),
+        ),
+        in_specs=[whole] * 4 + [far] * 3,
+        out_specs=(whole, whole),
+        scratch_shapes=[
+            pltpu.VMEM((room, size * width), bf16),
+            pltpu.VMEM(gate.shape, bf16),
+            pltpu.VMEM(up.shape, bf16),
+            pltpu.VMEM(down.shape, bf16),
+            pltpu.VMEM((size, share, 2 * hidden_width), bf16),
+            pltpu.VMEM((share, hidden_width), bf16),
+            pltpu.VMEM((room, inner), bf16),
+            pltpu.VMEM((room, size * width), bf16),
+            pltpu.SemaphoreType.DMA((3,)),
+        ]
+        + gather_sems(fast, slow, ROW_PIECES)
+        + gather_sems(fast, slow, 2)
+        + reduce_scratch(fast, slow, share, 2 * hidden_width, 4)
+        + reduce_scratch(fast, slow, room, width, 4),
+        compiler_params=pltpu.CompilerParams(
+            collective_id=collective_id, has_side_effects=True, vmem_limit_bytes=54 << 20
+        ),
+    )(rows, every_cols, dense_gate, dense_up, gate, up, down)
+
+
 def rms_norm(values, gain):
     flt = values.astype(jnp.float32)
     scaled = flt * lax.rsqrt(jnp.mean(flt * flt, axis=-1, keepdims=True) + 1e-06)
@@ -374,16 +683,16 @@
     route_weights = jax.nn.softmax(route_logits, axis=-1)
     top_count = route_ids.shape[1]
     side = jnp.concatenate(
-        [route_ids.astype(jnp.float32), route_weights, branch[:, None]], axis=1
+        [route_ids.astype(jnp.float32).T, route_weights.T, branch[None, :]], axis=0
     )
-    side = jnp.pad(side, ((0, 0), (0, 128 - side.shape[1])))
-    every_cols, every_side = all_gather([own_cols, side], "ep", ep_count, [1, 1], False, 2)
+    side = jnp.pad(side, ((0, -side.shape[0] % 8), (0, -seq_count % 128)))
+    every_cols, every_side = all_gather([own_cols, side], "ep", ep_count, [2, 1], False, 2)
     total_count = ep_count * seq_count
     every_cols = every_cols.reshape(total_count, part_width)
-    every_side = every_side.reshape(total_count, 128)
-    every_ids = every_side[:, :top_count]
-    every_weights = every_side[:, top_count : 2 * top_count]
-    every_branch = every_side[:, 2 * top_count]
+    every_side = every_side[:, :, :seq_count].transpose(1, 0, 2).reshape(-1, total_count)
+    every_ids = every_side[:top_count].T
+    every_weights = every_side[top_count : 2 * top_count].T
+    every_branch = every_side[2 * top_count]
     mine = every_ids == lax.axis_index("ep").astype(jnp.float32)
     taken = jnp.any(mine, axis=1)
     own_weight = jnp.sum(jnp.where(mine, every_weights, 0.0), axis=1)
@@ -394,23 +703,19 @@
     row_weight = jnp.sum(jnp.where(select, own_weight[None, :], 0.0), axis=1)
     select = select.astype(jnp.bfloat16)
     expert_in = jnp.dot(select, every_cols, preferred_element_type=jnp.float32).astype(jnp.bfloat16)
-    (full_rows,) = all_gather([expert_in], "tp", tp_count, [4], True, 3)
-    hidden_width = dense_gate.shape[1]
-    gate_part = jnp.dot(every_cols, dense_gate, preferred_element_type=jnp.float32)
-    up_part = jnp.dot(every_cols, dense_up, preferred_element_type=jnp.float32)
-    both = jnp.concatenate([gate_part.astype(jnp.bfloat16), up_part.astype(jnp.bfloat16)], axis=1)
-    both = both.reshape(tp_count, total_count // tp_count, 2 * hidden_width)
-    summed = reduce_scatter(both, "tp", tp_count, 4, False, 4).astype(jnp.float32)
-    own_hidden = (
-        jax.nn.silu(summed[:, :hidden_width]) * summed[:, hidden_width:]
-    ).astype(jnp.bfloat16)
-    (dense_hidden,) = all_gather([own_hidden], "tp", tp_count, [2], False, 5)
-    dense_hidden = dense_hidden.reshape(total_count, hidden_width)
-    gate_val = jnp.dot(full_rows, expert_gate[0], preferred_element_type=jnp.float32)
-    up_val = jnp.dot(full_rows, expert_up[0], preferred_element_type=jnp.float32)
-    hidden = (jax.nn.silu(gate_val) * up_val).astype(jnp.bfloat16)
-    expert_part = jnp.dot(hidden, expert_down[0], preferred_element_type=jnp.float32)
-    expert_cols = reduce_scatter(expert_part.astype(jnp.bfloat16), "tp", tp_count, 4, True, 6)
+    dense_hidden, expert_cols = branches(
+        expert_in,
+        every_cols,
+        dense_gate,
+        dense_up,
+        expert_gate[0],
+        expert_up[0],
+        expert_down[0],
+        "tp",
+        tp_count,
+        3,
+    )
+    dense_hidden = dense_hidden.reshape(total_count, dense_gate.shape[1])
     weighted = (expert_cols.astype(jnp.float32) * row_weight[:, None]).astype(jnp.bfloat16)
     routed_part = lax.dot_general(
         select, weighted, (((0,), (0,)), ((), ())), preferred_element_type=jnp.float32
@@ -418,7 +723,7 @@
     dense_part = jnp.dot(dense_hidden, dense_down, preferred_element_type=jnp.float32)
     share = (routed_part + every_branch[:, None] * dense_part).astype(jnp.bfloat16)
     share = share.reshape(ep_count, seq_count, part_width)
-    gathered = reduce_scatter(share, "ep", ep_count, 1, False, 7)
+    gathered = reduce_scatter(share, "ep", ep_count, 2, False, 4)
     resid_cols = lax.dynamic_slice_in_dim(resid, tp_index * part_width, part_width, 1)
     output = (resid_cols.astype(jnp.float32) + gathered.astype(jnp.float32)).astype(jnp.bfloat16)
     return (output, new_states)

time: 220 us -> 165 us (0.75)
  matrix products: 37.6 us -> 15.1 us
  Pallas kernels: 150 us -> 131 us
  local copies, waits for them, and re-layouts: 17.2 us -> 6.79 us
  other arithmetic: 13.3 us -> 10 us
    pallas_call x0 -> x1, Pallas kernels: none -> 60.2 us  [branches(): pl.pallas_call(functools.partial(branches_kernel, axis, size), out_shape=...]
    pallas_call x4 -> x2, Pallas kernels: 78 us -> 35.1 us  [reduce_scatter(): pl.pallas_call(functools.partial(reduce_kernel, axis, size, number, cols)...]
    pallas_call x4 -> x2, Pallas kernels: 72.4 us -> 35.9 us  [all_gather(): pl.pallas_call(functools.partial(gather_kernel, axis, size, pieces, cols)...]
    dot_general x4 -> x0, matrix products: 23.6 us -> none  [the longest x1 14.2 us: shards(): jnp.dot(hidden, expert_down[0], preferred_element_type=jnp.float32)]
    unnamed x45 -> x31, local copies, waits for them, and re-layouts: 8.03 us -> 1.96 us
    concatenate x2 -> x0, local copies, waits for them, and re-layouts: 4.37 us -> none  [the longest x1 4.27 us: shards(): jnp.concatenate([gate_part.astype(jnp.bfloat16), up_part.astype(jnp.bfloa...]
    transpose x0 -> x2, other arithmetic: none -> 2.52 us  [the longest x1 1.29 us: shards(): side = jnp.concatenate([route_ids.astype(jnp.float32).T, route_weights.T,...]
where the time goes in v2:
time: 165 us; the launch traced here: 164 us
  Pallas kernels  131 us (79%)
  matrix products  15.1 us (9%)
  other arithmetic  10 us (6%)
  local copies, waits for them, and re-layouts  6.79 us (4%)
    pallas_call x1, Pallas kernels, branches(): pl.pallas_call(functools.partial(branches_kernel, axis, size), out_shape=...  60.2 us
    pallas_call x2, Pallas kernels, all_gather(): pl.pallas_call(functools.partial(gather_kernel, axis, size, pieces, cols)...  35.9 us
    pallas_call x2, Pallas kernels, reduce_scatter(): pl.pallas_call(functools.partial(reduce_kernel, axis, size, number, cols)...  35.1 us

profile of v2, /device:TPU:0, one launch (start us, length us, event | category | flops | bytes accessed | tf_op | source)
XLA Modules:
  0.0 164.1 jit_solution(2018472023410874437)
XLA Ops:
  0.7 0.8 reduce_max.9
  1.5 0.7 fusion.47
  2.2 1.3 divide_bitcast_fusion
  3.5 0.7 exp.12
  4.1 1.4 fusion.3
  5.5 1.2 convert_bitcast_fusion
  6.8 0.8 mul.217
  7.5 0.7 reshape.99
  8.2 0.8 add_divide_fusion
  9.1 2.4 %convolution_convert_fusion.2 = bf16[96,256]{1,0:T(8,128)(2,1)S(1)} fusion(bf16[4096,256]{1,0:T(8,128)(2,1)} %param.26, bf16[96,4096]{1,0:T(8,128)(2,1)} %param.23, f32[4096]{0:T(1024)} %param.24, f32[96]{0:T(128)S(1)} %add_rsqrt_fusion.1), kind=kOutput, calls=%fused_computation.27 | convolution fusion | flops 202924032 | bytes 2949504 | tf_op jit(solution)/shard_map/dot_general | solution.py:668
  11.6 1.2 fusion.50
  13.0 1.0 copy.38
  14.0 2.0 %fusion.7 = f32[96,16,64]{0,2,1:T(8,128)S(1)} fusion(bf16[96,16,16]{0,2,1:T(8,128)(2,1)S(1)} %bitcast.73, f32[96,16,64]{0,2,1:T(8,128)S(1)} %bitcast.69, f32[96,16,64]{0,2,1:T(8,128)} %bitcast.71, f32[16,64]{1,0:T(8,128)S(1)} %get-tuple-element.17, f32[16,64]{1,0:T(8,128)S(1)} %get-tuple-element.15, f32[16,64,16]{1,2,0:T(8,128)} %param.30, ...), kind=kOutput, calls=%fused_computation.17 | convolution fusion | flops 19316736 | bytes 1376256 | tf_op jit(solution)/shard_map/ngh,gph->ngp/dot_general | solution.py:622
  16.1 1.9 %fusion.8 = f32[96,16,64]{0,2,1:T(8,128)S(1)} fusion(bf16[96,16,16]{0,2,1:T(8,128)(2,1)S(1)} %bitcast.74, f32[96,16,64]{0,2,1:T(8,128)S(1)} %bitcast.72, f32[96,16,64]{0,2,1:T(8,128)} %bitcast.70, f32[16,64]{1,0:T(8,128)S(1)} %get-tuple-element.17, f32[16,64]{1,0:T(8,128)S(1)} %get-tuple-element.15, f32[16,64,16]{1,2,0:T(8,128)S(1)} %copy-done.5, ...), kind=kOutput, calls=%fused_computation.19 | convolution fusion | flops 19316736 | bytes 1376256 | tf_op jit(solution)/shard_map/ngh,gph->ngp/dot_general | solution.py:621
  17.9 0.6 fusion.51
  18.5 0.6 fusion.14
  19.1 0.7 fusion.35
  20.2 0.9 pad_maximum_fusion
  21.1 0.5 convolution_convert_fusion.x_ref
  21.6 9.6 %shard_map.230.refs_0_ = bf16[96,1024]{1,0:T(8,128)(2,1)S(1)} custom-call(bf16[96,4096]{1,0:T(8,128)(2,1)S(1)} %convolution_convert_fusion.x_ref), custom_call_target="tpu_custom_call" | custom-call | tf_op jit(solution)/shard_map/pallas_call | solution.py:262
  31.2 8.2 %shard_map.231 = bf16[96,4096]{1,0:T(8,128)(2,1)S(1)} custom-call(bf16[96,1024]{1,0:T(8,128)(2,1)S(1)} %shard_map.230.refs_0_), custom_call_target="tpu_custom_call" | custom-call | tf_op jit(solution)/shard_map/pallas_call | solution.py:163
  39.4 0.4 fusion
  40.1 0.3 fusion.19
  40.5 27.7 %shard_map.232 = (bf16[8,96,1024]{2,1,0:T(8,128)(2,1)S(1)}, f32[8,8,128]{2,1,0:T(8,128)S(1)}) custom-call(bf16[96,1024]{1,0:T(8,128)(2,1)S(1)} %constant_dynamic-slice_fusion.refs_0_, f32[8,128]{1,0:T(8,128)S(1)} %select_maximum_fusion.refs_1_), custom_call_target="tpu_custom_call" | custom-call | tf_op jit(solution)/shard_map/pallas_call | solution.py:163
  68.2 1.1 copy-done.1
  70.3 0.3 select_reduce_fusion
  70.7 3.1 %convolution_convert_fusion.1.rows_ref = bf16[384,1024]{1,0:T(8,128)(2,1)} fusion(bf16[768,1024]{1,0:T(8,128)(2,1)} %bitcast.61, s32[768]{0:T(1024)S(1)} %add_bitcast_fusion, pred[768]{0:T(1024)(128)(4,1)S(1)} %reduce_or.12), kind=kOutput, calls=%fused_computation.15 | convolution fusion | flops 604962816 | bytes 2363136 | tf_op jit(solution)/shard_map/dot_general | solution.py:705
  73.7 60.2 %shard_map.233 = (bf16[4,192,768]{2,1,0:T(8,128)(2,1)}, bf16[384,1024]{1,0:T(8,128)(2,1)}) custom-call(bf16[384,1024]{1,0:T(8,128)(2,1)} %convolution_convert_fusion.1.rows_ref, bf16[768,1024]{1,0:T(8,128)(2,1)} %bitcast.62, bf16[1024,768]{1,0:T(8,128)(2,1)} %dense_gate.1, bf16[1024,768]{1,0:T(8,128)(2,1)} %dense_up.1, bf16[4096,768]{1,0:T(8,128)(2,1)} %bitcast.64, ...), custom_call_target="tpu_custom_call" | custom-call | tf_op jit(solution)/shard_map/pallas_call | solution.py:562
  133.9 2.4 %fusion.10 = f32[768,1024]{1,0:T(8,128)S(1)} fusion(bf16[384,1024]{1,0:T(8,128)(2,1)} %get-tuple-element.8, f32[384]{0:T(512)S(1)} %select_reduce_fusion, s32[768]{0:T(1024)S(1)} %add_bitcast_fusion, pred[768]{0:T(1024)(128)(4,1)S(1)} %reduce_or.12), kind=kOutput, calls=%fused_computation.23 | convolution fusion | flops 605749248 | bytes 3937536 | tf_op jit(solution)/shard_map/dot_general | solution.py:720
  136.4 1.4 add_convert_fusion
  137.8 25.6 %shard_map.234 = bf16[96,1024]{1,0:T(8,128)(2,1)S(1)} custom-call(bf16[8,96,1024]{2,1,0:T(8,128)(2,1)S(1)} %bitcast.63), custom_call_target="tpu_custom_call" | custom-call | tf_op jit(solution)/shard_map/pallas_call | solution.py:262
  163.3 0.7 add_convert_fusion.1
  (52 shorter events, 2.1 us)
Async XLA Ops:
  0.6 20.5 %copy-start = (bf16[256,4096]{1,0:T(8,128)(2,1)S(1)}, bf16[256,4096]{1,0:T(8,128)(2,1)}, u32[]{:S(2)}) copy-start(bf16[256,4096]{1,0:T(8,128)(2,1)} %param.36) | copy-start | bytes 6291460
  13.0 1.0 copy-start.2
  13.0 3.1 %copy-start.5 = (f32[16,64,16]{1,2,0:T(8,128)S(1)}, f32[16,64,16]{1,2,0:T(8,128)}, u32[]{:S(2)}) copy-start(f32[16,64,16]{1,2,0:T(8,128)} %param.31) | copy-start | bytes 196612
  13.0 3.1 %copy-start.6 = (f32[16,64,16]{1,2,0:T(8,128)S(1)}, f32[16,64,16]{1,2,0:T(8,128)}, u32[]{:S(2)}) copy-start(f32[16,64,16]{1,2,0:T(8,128)} %param.30) | copy-start | bytes 196612
  14.0 2.1 %copy-start.3 = (f32[1,96,1024]{1,2,0:T(8,128)S(1)}, f32[1,96,1024]{1,2,0:T(8,128)}, u32[]{:S(2)}) copy-start(f32[1,96,1024]{1,2,0:T(8,128)} %copy.38) | copy-start | bytes 1179652
  14.0 3.9 %copy-start.9 = (f32[16,16,64]{2,1,0:T(8,128)S(1)}, f32[16,16,64]{2,1,0:T(8,128)}, u32[]{:S(2)}) copy-start(f32[16,16,64]{2,1,0:T(8,128)} %param.32) | copy-start | bytes 196612
  16.1 2.5 %copy-start.8 = (f32[16,16,64]{2,1,0:T(8,128)S(1)}, f32[16,16,64]{2,1,0:T(8,128)}, u32[]{:S(2)}) copy-start(f32[16,16,64]{2,1,0:T(8,128)} %param.33) | copy-start | bytes 196612
  20.0 1.1 copy-start.7
  21.6 17.8 %copy-start.4 = (bf16[96,4096]{1,0:T(8,128)(2,1)S(1)}, bf16[96,4096]{1,0:T(8,128)(2,1)}, u32[]{:S(2)}) copy-start(bf16[96,4096]{1,0:T(8,128)(2,1)} %param.23) | copy-start | bytes 2359300
  31.2 8.6 %copy-start.10 = (f32[4096]{0:T(1024)S(1)}, f32[4096]{0:T(1024)}, u32[]{:S(2)}) copy-start(f32[4096]{0:T(1024)} %param.25) | copy-start | bytes 49156
  39.8 0.7 copy-start.11
  39.8 0.7 copy-start.12
  68.2 1.2 copy-start.1
  133.9 2.4 %copy-start.13 = (bf16[768,1024]{1,0:T(8,128)(2,1)S(1)}, bf16[768,1024]{1,0:T(8,128)(2,1)}, u32[]{:S(2)}) copy-start(bf16[768,1024]{1,0:T(8,128)(2,1)} %param.44) | copy-start | bytes 4718596
  133.9 2.4 %copy-start.14 = (bf16[4,192,768]{2,1,0:T(8,128)(2,1)S(1)}, bf16[4,192,768]{2,1,0:T(8,128)(2,1)}, u32[]{:S(2)}) copy-start(bf16[4,192,768]{2,1,0:T(8,128)(2,1)} %get-tuple-element.9) | copy-start | bytes 3538948
